TPU v7x, 32 devices: a whole 2x2x4 slice. The times are simulated.
32 devices in a mesh: fs: 16 (over z, y, core), tp: 2 (over x).
Axes of the slice: x: 2, y: 2, z: 4, core: 2. Of those that a mesh axis runs over, the one named last changes fastest.
Arguments:
- tokens: bfloat16 [6144, 2048], P('fs', 'tp'), may hold values from -60 to 60
- gain_mixer: float32 [2048], P('tp'), may hold values from 0.1 to 1.9
- w_in: bfloat16 [2048, 1024], P('fs', 'tp'), may hold values from -0.125 to 0.125
- pool_scale: float32 [1024], P('tp'), may hold values from 0.1 to 1.9
- w_pool_out: bfloat16 [2048, 1024], P('fs', 'tp'), may hold values from -0.25 to 0.25
- gain_mid: float32 [2048], P('tp'), may hold values from 0.1 to 1.9
- w_ff1: bfloat16 [2048, 8192], P('fs', 'tp'), may hold values from -0.125 to 0.125
- w_ff2: bfloat16 [2048, 8192], P('fs', 'tp'), may hold values from -0.09375 to 0.09375
- gain_out: float32 [2048], P('tp'), may hold values from 0.1 to 1.9
Outputs:
- layer_out: bfloat16 [6144, 2048], P('fs', 'tp')
All inputs are finite; a program needn't handle non-finite values.
Results may differ from a plain program's by a relative error of at most 0.017.
Values may be sent and summed in bfloat16 or wider, within the bound.
A program may use at most 128 MiB of HBM per device.

v0:
```python
import jax
import jax.numpy as jnp
from jax import lax
from jax.sharding import PartitionSpec as P

norm_eps = 1e-05
residual_alpha = 2.0**0.25


def row_norm(value, gain):
    width = value.shape[1] * lax.axis_size("tp")
    total, squares = lax.psum((jnp.sum(value, axis=1), jnp.sum(value * value, axis=1)), "tp")
    mean = (total / width)[:, None]
    spread = (squares / width)[:, None] - mean * mean
    return (value - mean) * lax.rsqrt(spread + norm_eps) * gain


def shifted(value, steps):
    return jnp.pad(value, ((steps, 0), (0, 0)))[: value.shape[0]]


def project_rows(weight, left):
    return lax.dot_general(
        weight, left, (((1,), (1,)), ((), ())), preferred_element_type=jnp.float32
    )


def fold_features(weight, piece):
    return jnp.dot(piece, weight, preferred_element_type=jnp.float32)


def local(tokens, gain_mixer, w_in, pool_scale, w_pool_out, gain_mid, w_ff1, w_ff2, gain_out):
    xf = tokens.astype(jnp.float32)
    length = tokens.shape[0]
    mixed_in = row_norm(xf, gain_mixer).astype(jnp.bfloat16)
    in_full = lax.all_gather(w_in, "fs", axis=0, tiled=True)
    channels = w_in.shape[1]
    pool_in = fold_features(in_full, lax.all_gather(mixed_in, "tp", axis=1, tiled=True))
    uf = pool_in.astype(jnp.bfloat16).astype(jnp.float32)
    group_width = channels * lax.axis_size("tp") // 4
    channel = lax.axis_index("tp") * channels + jnp.arange(channels, dtype=jnp.int32)
    group = channel // group_width
    sum_two = uf + shifted(uf, 1)
    sum_four = sum_two + shifted(sum_two, 2)
    sum_eight = sum_four + shifted(sum_four, 4)
    sum_sixteen = sum_eight + shifted(sum_eight, 8)
    window_sum = jnp.where(
        group == 0,
        sum_two,
        jnp.where(group == 1, sum_four, jnp.where(group == 2, sum_eight, sum_sixteen)),
    )
    window = jnp.where(
        group == 0, 2.0, jnp.where(group == 1, 4.0, jnp.where(group == 2, 8.0, 16.0))
    ).astype(jnp.float32)
    position = jnp.arange(length, dtype=jnp.float32)[:, None]
    count = jnp.minimum(position + 1.0, window[None, :])
    pooled = ((window_sum / count - uf) * pool_scale).astype(jnp.bfloat16)
    out_full = lax.all_gather(w_pool_out, "fs", axis=0, tiled=True)
    mixer_out = lax.psum_scatter(
        project_rows(out_full, pooled).astype(jnp.bfloat16), "tp", scatter_dimension=0, tiled=True
    ).astype(jnp.float32)
    mixer_out = mixer_out.astype(jnp.bfloat16).T
    middle = row_norm(residual_alpha * xf + mixer_out.astype(jnp.float32), gain_mid).astype(
        jnp.bfloat16
    )
    up_full = lax.all_gather(w_ff1, "fs", axis=0, tiled=True)
    upward = fold_features(up_full, lax.all_gather(middle, "tp", axis=1, tiled=True))
    hidden = jnp.square(jax.nn.relu(upward)).astype(jnp.bfloat16)
    down_full = lax.all_gather(w_ff2, "fs", axis=0, tiled=True)
    ff_out = lax.psum_scatter(
        project_rows(down_full, hidden).astype(jnp.bfloat16), "tp", scatter_dimension=0, tiled=True
    ).astype(jnp.float32)
    ff_out = ff_out.astype(jnp.bfloat16).T
    result = row_norm(
        residual_alpha * middle.astype(jnp.float32) + ff_out.astype(jnp.float32), gain_out
    )
    return result.astype(jnp.bfloat16)


def solution(mesh):
    return jax.shard_map(
        local,
        mesh=mesh,
        in_specs=(
            P("fs", "tp"),
            P("tp"),
            P("fs", "tp"),
            P("tp"),
            P("fs", "tp"),
            P("tp"),
            P("fs", "tp"),
            P("fs", "tp"),
            P("tp"),
        ),
        out_specs=P("fs", "tp"),
        check_vma=False,
    )
```

profile of v0, /device:TPU:0, one launch (start us, length us, event | category | flops | bytes accessed | tf_op | source)
XLA Modules:
  0.0 509.2 jit_solution(2410414311106388984)
XLA Ops:
  6.5 0.0 all-gather.7.cloned.1.call-start
  6.5 1.4 convert_reduce_fusion
  8.0 5.9 %all-reduce.6 = (f32[384]{0:T(512)S(1)}, f32[384]{0:T(512)S(1)}) all-reduce(f32[384]{0:T(512)S(1)} %get-tuple-element.10, f32[384]{0:T(512)S(1)} %get-tuple-element.9), channel_id=1, replica_groups=mesh['fs'=16,'tp'=2] {'tp'}, use_global_device_ids=true, to_apply=%region_3.0 | all-reduce | flops 768 | bytes 6144 | tf_op jit(solution)/shard_map/psum | solution.py:12
  13.9 2.3 fusion.7
  16.2 0.0 all-gather.7.cloned.1.call-update
  16.2 0.0 all-gather.9.cloned.1.call-start
  16.3 0.7 all-gather.9.cloned.1.call-update
  17.0 0.0 all-gather.11.cloned.1.call-start
  17.0 0.7 all-gather.11.cloned.1.call-update
  17.7 0.0 reduce-scatter.3.cloned.1.call-start
  17.8 27.5 %all-gather.7.cloned.1.call-done = bf16[384,2048]{1,0:T(8,128)(2,1)} async-done(((bf16[384,1024]{1,0:T(8,128)(2,1)}), bf16[384,2048]{1,0:T(8,128)(2,1)}) %all-gather.7.cloned.1.call-update) | async-done | bytes 1572880 | tf_op jit(solution)/shard_map/all_gather | solution.py:38
  45.3 43.7 %all-gather.9.cloned.1.call-done = bf16[2048,512]{1,0:T(8,128)(2,1)} async-done(((bf16[128,512]{1,0:T(8,128)(2,1)}), bf16[2048,512]{1,0:T(8,128)(2,1)}) %all-gather.9.cloned.1.call-update) | async-done | bytes 2097168 | tf_op jit(solution)/shard_map/all_gather | solution.py:36
  89.0 3.0 fusion.9
  92.0 0.1 fusion.12
  92.2 0.0 copy-start.6
  92.2 0.1 fusion.13
  92.3 0.1 fusion.14
  92.4 39.0 %all-gather.11.cloned.1.call-done = bf16[2048,512]{1,0:T(8,128)(2,1)} async-done(((bf16[128,512]{1,0:T(8,128)(2,1)}), bf16[2048,512]{1,0:T(8,128)(2,1)}) %all-gather.11.cloned.1.call-update) | async-done | bytes 2097168 | tf_op jit(solution)/shard_map/all_gather | solution.py:58
  131.4 0.0 copy-done.6
  131.4 3.9 fusion.2
  135.3 0.0 copy-start
  135.3 0.0 reduce-scatter.3.cloned.1.call-update
  135.3 0.0 all-gather.13.cloned.1.call-start
  135.4 25.0 %reduce-scatter.3.cloned.1.call-done = bf16[1024,384]{0,1:T(8,128)(2,1)} async-done(((bf16[2048,384]{0,1:T(8,128)(2,1)}), bf16[1024,384]{0,1:T(8,128)(2,1)}) %reduce-scatter.3.cloned.1.call-update) | async-done | bytes 786448 | tf_op jit(solution)/shard_map/reduce_scatter | solution.py:59
  160.3 0.0 copy-done
  160.4 1.7 fusion.11
  162.0 4.9 all-reduce.5
  167.0 0.0 copy-done.4
  167.0 0.0 copy-done.2
  167.0 1.3 multiply_convert_fusion.2
  168.3 0.0 all-gather.13.cloned.1.call-update
  168.3 0.0 all-gather.15.cloned.1.call-start
  168.3 0.5 all-gather.15.cloned.1.call-update
  168.9 0.0 all-gather.17.cloned.1.call-start
  168.9 0.7 all-gather.17.cloned.1.call-update
  169.6 0.0 reduce-scatter.5.cloned.1.call-start
  169.7 26.0 %all-gather.13.cloned.1.call-done = bf16[384,2048]{1,0:T(8,128)(2,1)} async-done(((bf16[384,1024]{1,0:T(8,128)(2,1)}), bf16[384,2048]{1,0:T(8,128)(2,1)}) %all-gather.13.cloned.1.call-update) | async-done | bytes 1572880 | tf_op jit(solution)/shard_map/all_gather | solution.py:67
  195.6 128.5 %all-gather.15.cloned.1.call-done = bf16[2048,4096]{1,0:T(8,128)(2,1)} async-done(((bf16[128,4096]{1,0:T(8,128)(2,1)}), bf16[2048,4096]{1,0:T(8,128)(2,1)}) %all-gather.15.cloned.1.call-update) | async-done | bytes 16777232 | tf_op jit(solution)/shard_map/all_gather | solution.py:66
  324.1 126.8 %all-gather.17.cloned.1.call-done = bf16[2048,4096]{1,0:T(8,128)(2,1)} async-done(((bf16[128,4096]{1,0:T(8,128)(2,1)}), bf16[2048,4096]{1,0:T(8,128)(2,1)}) %all-gather.17.cloned.1.call-update) | async-done | bytes 16777232 | tf_op jit(solution)/shard_map/all_gather | solution.py:69
  450.9 19.0 %fusion.3 = bf16[2048,384]{0,1:T(8,128)(2,1)} fusion(bf16[2048,4096]{1,0:T(8,128)(2,1)} %all-gather.17.cloned.1.call-done, bf16[384,2048]{1,0:T(8,128)(2,1)} %all-gather.13.cloned.1.call-done, bf16[2048,4096]{1,0:T(8,128)(2,1)} %all-gather.15.cloned.1.call-done), kind=kOutput, calls=%fused_computation.9 | convolution fusion | flops 12890406912 | bytes 36700160 | tf_op jit(solution)/shard_map/dot_general | solution.py:23
  469.9 0.0 reduce-scatter.5.cloned.1.call-update
  470.0 24.5 %reduce-scatter.5.cloned.1.call-done = bf16[1024,384]{0,1:T(8,128)(2,1)} async-done(((bf16[2048,384]{0,1:T(8,128)(2,1)}), bf16[1024,384]{0,1:T(8,128)(2,1)}) %reduce-scatter.5.cloned.1.call-update) | async-done | bytes 786448 | tf_op jit(solution)/shard_map/reduce_scatter | solution.py:70
  494.4 0.0 copy-done.1
  494.4 1.7 fusion.10
  496.1 4.9 all-reduce.4
  501.0 0.0 copy-done.5
  501.0 0.0 copy-done.3
  501.1 1.3 multiply_convert_fusion.1
  (12 shorter events, 0.1 us)
Async XLA Ops:
  6.5 38.8 %all-gather.7.cloned.1.call-start = ((), (), s32[]{:S(2)}) async-start(), calls=%async_computation.2 | async-start | bytes 2359296 | tf_op jit(solution)/shard_map/all_gather | solution.py:38
  16.2 72.8 %all-gather.9.cloned.1.call-start = ((), (), s32[]{:S(2)}) async-start(), calls=%async_computation.3 | async-start | bytes 2228224 | tf_op jit(solution)/shard_map/all_gather | solution.py:36
  17.0 114.4 %all-gather.11.cloned.1.call-start = ((), (), s32[]{:S(2)}) async-start(), calls=%async_computation.4 | async-start | bytes 2228224 | tf_op jit(solution)/shard_map/all_gather | solution.py:58
  17.7 142.7 %reduce-scatter.3.cloned.1.call-start = ((), (), s32[]{:S(2)}) async-start(), calls=%async_computation.5 | async-start | bytes 2359296 | tf_op jit(solution)/shard_map/reduce_scatter | solution.py:59
  92.2 39.2 %copy-start.6 = (f32[512]{0:T(512)S(1)}, f32[512]{0:T(512)}, u32[]{:S(2)}) copy-start(f32[512]{0:T(512)} %param.12) | copy-start | bytes 6148
  135.3 25.0 %copy-start = (bf16[384,1024]{1,0:T(8,128)(2,1)S(1)}, bf16[384,1024]{1,0:T(8,128)(2,1)}, u32[]{:S(2)}) copy-start(bf16[384,1024]{1,0:T(8,128)(2,1)} %param.9) | copy-start | bytes 2359300
  135.3 31.6 %copy-start.4 = (f32[1024]{0:T(1024)S(1)}, f32[1024]{0:T(1024)}, u32[]{:S(2)}) copy-start(f32[1024]{0:T(1024)} %param.14) | copy-start | bytes 12292
  135.3 60.3 %all-gather.13.cloned.1.call-start = ((), (), s32[]{:S(2)}) async-start(), calls=%async_computation.6 | async-start | bytes 2359296 | tf_op jit(solution)/shard_map/all_gather | solution.py:67
  160.3 6.6 %copy-start.2 = (bf16[1024,384]{0,1:T(8,128)(2,1)S(1)}, bf16[1024,384]{0,1:T(8,128)(2,1)}, u32[]{:S(2)}) copy-start(bf16[1024,384]{0,1:T(8,128)(2,1)} %reduce-scatter.3.cloned.1.call-done) | copy-start | bytes 2359300
  168.3 155.8 %all-gather.15.cloned.1.call-start = ((), (), s32[]{:S(2)}) async-start(), calls=%async_computation.7 | async-start | bytes 17825792 | tf_op jit(solution)/shard_map/all_gather | solution.py:66
  168.9 282.1 %all-gather.17.cloned.1.call-start = ((), (), s32[]{:S(2)}) async-start(), calls=%async_computation.8 | async-start | bytes 17825792 | tf_op jit(solution)/shard_map/all_gather | solution.py:69
  169.6 324.8 %reduce-scatter.5.cloned.1.call-start = ((), (), s32[]{:S(2)}) async-start(), calls=%async_computation.9 | async-start | bytes 2359296 | tf_op jit(solution)/shard_map/reduce_scatter | solution.py:70
  469.9 24.5 %copy-start.1 = (bf16[384,1024]{1,0:T(8,128)(2,1)S(1)}, bf16[384,1024]{1,0:T(8,128)(2,1)}, u32[]{:S(2)}) copy-start(bf16[384,1024]{1,0:T(8,128)(2,1)} %multiply_convert_fusion.2) | copy-start | bytes 2359300
  469.9 31.1 %copy-start.5 = (f32[1024]{0:T(1024)S(1)}, f32[1024]{0:T(1024)}, u32[]{:S(2)}) copy-start(f32[1024]{0:T(1024)} %param.17) | copy-start | bytes 12292
  494.4 6.6 %copy-start.3 = (bf16[1024,384]{0,1:T(8,128)(2,1)S(1)}, bf16[1024,384]{0,1:T(8,128)(2,1)}, u32[]{:S(2)}) copy-start(bf16[1024,384]{0,1:T(8,128)(2,1)} %reduce-scatter.5.cloned.1.call-done) | copy-start | bytes 2359300
Sparse Core Ops, SparseCore 0:
  16.3 28.9 all-gather.6
  47.5 41.4 all-gather.8
  91.2 40.1 all-gather.10
  135.5 24.8 reduce-scatter.2
  168.4 27.1 all-gather.12
  197.7 126.4 all-gather.14
  326.3 124.5 all-gather.16
  470.1 24.3 reduce-scatter.4
where the time goes:
time: 510 us; the launch traced here: 509 us
  waiting for transfers between devices  444 us (87%)
  matrix products  26 us (5%)
  blocking collectives  15.7 us (3%)
  between operations  13.6 us (3%)
  other arithmetic  10 us (2%)
    all_gather x1, waiting for transfers between devices, local(): up_full = lax.all_gather(w_ff1, 'fs', axis=0, tiled=True)  128 us
    all_gather x1, waiting for transfers between devices, local(): down_full = lax.all_gather(w_ff2, 'fs', axis=0, tiled=True)  127 us
    all_gather x1, waiting for transfers between devices, local(): in_full = lax.all_gather(w_in, 'fs', axis=0, tiled=True)  43.7 us
    all_gather x1, waiting for transfers between devices, local(): out_full = lax.all_gather(w_pool_out, 'fs', axis=0, tiled=True)  39 us
    all_gather x1, waiting for transfers between devices, local(): lax.all_gather(mixed_in, 'tp', axis=1, tiled=True)  27.5 us
    all_gather x1, waiting for transfers between devices, local(): lax.all_gather(middle, 'tp', axis=1, tiled=True)  26 us
    reduce_scatter x1, waiting for transfers between devices, local(): lax.psum_scatter(project_rows(out_full, pooled).astype(jnp.bfloat16), 'tp...  25 us
    reduce_scatter x1, waiting for transfers between devices, local(): lax.psum_scatter(project_rows(down_full, hidden).astype(jnp.bfloat16), 't...  24.5 us
  transfers between devices with their start and end apart: 8, of which 8 were waited for; matrix products, arithmetic and copies ran while one was open for 1% of the time, Pallas kernels for 0%

commit v1 on v0

v1 whole, which is shorter than its diff:
```python
import functools
import math

import jax
import jax.numpy as jnp
from jax import lax
from jax.experimental import pallas as pl
from jax.experimental.pallas import tpu as pltpu
from jax.sharding import PartitionSpec as P

norm_eps = 1e-05
residual_alpha = 2.0**0.25
f32, bf16 = jnp.float32, jnp.bfloat16
MESH = pl.DeviceIdType.MESH


def nt_dot(left, right):
    return lax.dot_general(left, right, (((1,), (1,)), ((), ())), preferred_element_type=f32)


def kernel(
    n, tps,
    x_ref, gains_ref, scale_ref, gout_ref, win_ref, wpo_ref, wup_ref, wdn_ref, out_ref,
    win, wpo, wup, wdn, xfull, gfull, mixed, mpart, mrecv, middle, hidden, part, precv, work,
    load_sem, is_sem, ir_sem, ds_sem, dr_sem, xs_sem, xr_sem, gs_sem, gr_sem,
    ms_sem, mr_sem, ps_sem, pr_sem,
):
    i, t = lax.axis_index("fs"), lax.axis_index("tp")
    core, chip = lax.rem(i, 2), lax.div(i, 2)
    half = n // 2
    rows, feat = x_ref.shape
    cin = win_ref.shape[1]
    width = feat * tps
    own = win_ref.shape[0]
    rh = own // 2
    rc = own * 2
    ffw = wup_ref.shape[1]
    fh = ffw // 2

    pos = jnp.where(lax.rem(chip, 2) == 0, lax.div(chip, 2), n - 1 - lax.div(chip, 2))

    def chip_at(p):
        q = lax.rem(p + 2 * n, n)
        return jnp.where(q < half, 2 * q, 2 * (n - 1 - q) + 1)

    sib = chip * 2 + (1 - core)
    ring = [chip_at(pos + 1) * 2 + core, chip_at(pos - 1) * 2 + core]
    peers = [lax.rem(t + q, tps) for q in range(1, tps)]

    streams = [(win, 0, cin), (wpo, 0, cin), (wup, 0, fh), (wup, fh, fh), (wdn, 0, fh), (wdn, fh, fh)]

    def block(w, where, c, d):
        ref, c0, cw = streams[w]
        r0 = pl.multiple_of((where * 2 + c) * own + d * rh, rh)
        return ref.at[pl.ds(r0, rh), pl.ds(c0, cw)]

    def source(s, d):
        return chip_at(pos - s) if d == 0 else chip_at(pos + s)

    def hop(w, s, d):
        b = block(w, source(s, d), core, d)
        return pltpu.make_async_remote_copy(
            b, b, is_sem.at[w, s, d], ir_sem.at[w, s, d], device_id=(ring[d], t), device_id_type=MESH)

    def share(w, s, d):
        b = block(w, source(s, d), core, d)
        return pltpu.make_async_remote_copy(
            b, b, ds_sem.at[w, s, d], dr_sem.at[w, s, d], device_id=(sib, t), device_id_type=MESH)

    def begin(w):
        for d in range(2):
            hop(w, 0, d).start()
        for d in range(2):
            share(w, 0, d).start()

    def advance(ws, s, last=False):
        for w in ws:
            for d in range(2):
                hop(w, s, d).wait_recv()
                if not last:
                    hop(w, s + 1, d).start()
                share(w, s + 1, d).start()

    def run(ws, lo, hi):
        def body(s, carry):
            advance(ws, s)
            return carry
        lax.fori_loop(lo, hi, body, 0)

    def shared(w):
        def body(s, carry):
            for d in range(2):
                share(w, s, d).wait_recv()
            return carry
        lax.fori_loop(0, n, body, 0)

    barrier = pltpu.get_barrier_semaphore()
    for f in ring + [sib]:
        pl.semaphore_signal(barrier, inc=1, device_id=(f, t), device_id_type=MESH)
    for p in peers:
        pl.semaphore_signal(barrier, inc=1, device_id=(i, p), device_id_type=MESH)
    loads = []
    mine = pl.ds(pl.multiple_of(i * own, own), own)
    for k, (src, dst) in enumerate(((win_ref, win), (wpo_ref, wpo), (wup_ref, wup), (wdn_ref, wdn))):
        loads.append(pltpu.make_async_copy(src, dst.at[mine], load_sem.at[k]))
        loads[-1].start()
    pl.semaphore_wait(barrier, 3 + len(peers))

    def x_copy(q):
        return pltpu.make_async_remote_copy(
            x_ref, xfull.at[t], xs_sem.at[q], xr_sem.at[q], device_id=(i, peers[q]), device_id_type=MESH)

    def g_copy(q):
        return pltpu.make_async_remote_copy(
            gains_ref, gfull.at[t], gs_sem.at[q], gr_sem.at[q], device_id=(i, peers[q]), device_id_type=MESH)

    for w in range(2):
        loads[w].wait()
        begin(w)
    for q in range(tps - 1):
        x_copy(q).start()
        g_copy(q).start()
    xfull[t] = x_ref[...]
    gfull[t] = gains_ref[...]

    run((0, 1), 0, n - 2)
    loads[2].wait()
    begin(2)
    begin(3)
    advance((0, 1), n - 2, last=True)
    loads[3].wait()

    rb = math.gcd(rows, 32)

    def blocks_of(body):
        def step(r, carry):
            body(pl.ds(pl.multiple_of(r * rb, rb), rb))
            return carry
        lax.fori_loop(0, rows // rb, step, 0)

    def norm(pieces):
        total = sum(jnp.sum(v, axis=1, keepdims=True) for v in pieces)
        mean = total / width
        pieces = [v - mean for v in pieces]
        spread = sum(jnp.sum(v * v, axis=1, keepdims=True) for v in pieces) / width
        inv = lax.rsqrt(spread + norm_eps)
        return [v * inv for v in pieces]

    for q in range(tps - 1):
        x_copy(q).wait_recv()
        g_copy(q).wait_recv()

    def first_norm(rs):
        pieces = norm([xfull[r, rs, :].astype(f32) for r in range(tps)])
        for r in range(tps):
            mixed[rs, r * feat:(r + 1) * feat] = (pieces[r] * gfull[r, 0:1, :]).astype(bf16)

    blocks_of(first_norm)
    shared(0)
    cb = math.gcd(cin, 128)
    gw = cin * tps // 4
    pool = jnp.dot(mixed[...], win[...], preferred_element_type=f32)
    work[:, :cin] = pool.astype(bf16).astype(f32)
    row = lax.broadcasted_iota(jnp.int32, (rows, cb), 0)
    position = (row + 1).astype(f32)
    pooled = []
    for c in range(cin // cb):
        cs = slice(c * cb, (c + 1) * cb)
        u = work[:, cs]

        def shifted(v, steps):
            return jnp.where(row >= steps, pltpu.roll(v, steps, axis=0), 0.0)

        s2 = u + shifted(u, 1)
        s4 = s2 + shifted(s2, 2)
        s8 = s4 + shifted(s4, 4)
        s16 = s8 + shifted(s8, 8)
        channel = t * cin + c * cb + lax.broadcasted_iota(jnp.int32, (rows, cb), 1)

        def pick(a, b, e, g):
            return jnp.where(channel < gw, a, jnp.where(channel < 2 * gw, b, jnp.where(channel < 3 * gw, e, g)))

        count = jnp.minimum(position, pick(2.0, 4.0, 8.0, 16.0))
        mixed[:, cs] = ((pick(s2, s4, s8, s16) / count - u) * scale_ref[0:1, cs]).astype(bf16)

    def m_copy(q):
        return pltpu.make_async_remote_copy(
            mpart, mrecv.at[q], ms_sem.at[q], mr_sem.at[q], device_id=(i, peers[q]), device_id_type=MESH)

    shared(1)
    wb = math.gcd(width, 512)

    def out_proj(k, carry):
        cs = pl.ds(pl.multiple_of(k * wb, wb), wb)
        mpart[:, cs] = nt_dot(mixed[:, :cin], wpo[cs, :]).astype(bf16)
        return carry

    lax.fori_loop(0, width // wb, out_proj, 0)
    for q in range(tps - 1):
        m_copy(q).start()

    run((2, 3), 0, half)
    for q in range(tps - 1):
        m_copy(q).wait_recv()

    def second_norm(rs):
        pieces = []
        for r in range(tps):
            cs = slice(r * feat, (r + 1) * feat)
            mix = mpart[rs, cs].astype(f32)
            for q in range(tps - 1):
                mix = mix + mrecv[q, rs, cs].astype(f32)
            mix = mix.astype(bf16).astype(f32)
            pieces.append(residual_alpha * xfull[r, rs, :].astype(f32) + mix)
        pieces = norm(pieces)
        for r in range(tps):
            middle[rs, r * feat:(r + 1) * feat] = (pieces[r] * gfull[r, 1:2, :]).astype(bf16)

    blocks_of(second_norm)
    run((2, 3), half, n - 2)
    begin(4)
    begin(5)
    advance((2, 3), n - 2, last=True)
    shared(2)
    shared(3)

    hb = math.gcd(ffw, 512)
    chunks = ffw // hb

    def up(k, carry):
        cs = pl.ds(pl.multiple_of(k * hb, hb), hb)
        act = jnp.maximum(jnp.dot(middle[...], wup[:, cs], preferred_element_type=f32), 0.0)
        hidden[:, cs] = (act * act).astype(bf16)
        return carry

    third = -(-chunks // 3)
    lax.fori_loop(0, third, up, 0)
    advance((4,), 0)
    lax.fori_loop(third, min(2 * third, chunks), up, 0)
    advance((5,), 0)
    lax.fori_loop(min(2 * third, chunks), chunks, up, 0)

    def p_copy(q, k):
        return pltpu.make_async_remote_copy(
            part.at[k], precv.at[q, k], ps_sem.at[q, k], pr_sem.at[q, k],
            device_id=(i, peers[q]), device_id_type=MESH)

    def down(distance):
        for w in (4, 5):
            share(w, distance, 0).wait_recv()
            share(w, lax.rem(n - distance, n), 1).wait_recv()
        k = chip_at(pos - distance)
        part[k] = nt_dot(hidden[...], wdn[pl.ds(pl.multiple_of(k * rc, rc), rc), :]).astype(bf16)
        for q in range(tps - 1):
            p_copy(q, k).start()

    advance((4, 5), 1)
    run((4, 5), 2, half - 1)

    def first_two(j, carry):
        down(j * half)
        return carry

    def last_two(s):
        def body(j, carry):
            down(jnp.where(j == 0, s + 1, n - 1 - s))
            return carry
        lax.fori_loop(0, 2, body, 0)

    advance((4, 5), half - 1)
    lax.fori_loop(0, 2, first_two, 0)

    def tail(s, carry):
        advance((4, 5), s)
        last_two(s)
        return carry

    lax.fori_loop(half, n - 2, tail, 0)
    advance((4, 5), n - 2, last=True)
    last_two(n - 2)

    for q in range(tps - 1):
        def arrived(k, carry):
            p_copy(q, k).wait_recv()
            return carry
        lax.fori_loop(0, n, arrived, 0)

    per = n // tps

    def last_norm(rs):
        total = jnp.zeros((rb, 1), f32)
        values = []
        for k in range(n):
            ff = part[k, rs, :].astype(f32)
            for q in range(tps - 1):
                ff = ff + precv[q, k, rs, :].astype(f32)
            v = residual_alpha * middle[rs, k * rc:(k + 1) * rc].astype(f32) + ff.astype(bf16).astype(f32)
            values.append(v)
            total = total + jnp.sum(v, axis=1, keepdims=True)
        mean = total / width
        square = jnp.zeros((rb, 1), f32)
        for v in values:
            square = square + jnp.sum((v - mean) * (v - mean), axis=1, keepdims=True)
        inv = lax.rsqrt(square / width + norm_eps)
        for j in range(per):
            v = values[j]
            for r in range(1, tps):
                v = jnp.where(t == r, values[r * per + j], v)
            cs = slice(j * rc, (j + 1) * rc)
            out_ref[rs, cs] = ((v - mean) * inv * gout_ref[0:1, cs]).astype(bf16)

    blocks_of(last_norm)

    for q in range(tps - 1):
        x_copy(q).wait_send()
        g_copy(q).wait_send()
        m_copy(q).wait_send()

        def sent(k, carry):
            p_copy(q, k).wait_send()
            return carry
        lax.fori_loop(0, n, sent, 0)

    def drained(s, carry):
        for w in range(len(streams)):
            for d in range(2):
                hop(w, s, d).wait_send()
                share(w, s, d).wait_send()
        return carry

    lax.fori_loop(0, n - 1, drained, 0)
    for w in range(len(streams)):
        for d in range(2):
            share(w, n - 1, d).wait_send()


def local(n, tps, tokens, gain_mixer, w_in, pool_scale, w_pool_out, gain_mid, w_ff1, w_ff2, gain_out):
    rows, feat = tokens.shape
    own, cin = w_in.shape
    ffw = w_ff1.shape[1]
    width = feat * tps
    rc = own * 2
    gains = jnp.stack([gain_mixer, gain_mid])
    vmem, hbm = pl.BlockSpec(memory_space=pltpu.VMEM), pl.BlockSpec(memory_space=pl.ANY)
    dma = pltpu.SemaphoreType.DMA
    lanes = tps - 1
    return pl.pallas_call(
        functools.partial(kernel, n, tps),
        out_shape=jax.ShapeDtypeStruct((rows, feat), bf16),
        in_specs=[vmem] * 4 + [hbm] * 4,
        out_specs=vmem,
        scratch_shapes=[
            pltpu.VMEM((width, cin), bf16),
            pltpu.VMEM((width, cin), bf16),
            pltpu.VMEM((width, ffw), bf16),
            pltpu.VMEM((width, ffw), bf16),
            pltpu.VMEM((tps, rows, feat), bf16),
            pltpu.VMEM((tps, 2, feat), f32),
            pltpu.VMEM((rows, width), bf16),
            pltpu.VMEM((rows, width), bf16),
            pltpu.VMEM((lanes, rows, width), bf16),
            pltpu.VMEM((rows, width), bf16),
            pltpu.VMEM((rows, ffw), bf16),
            pltpu.VMEM((n, rows, rc), bf16),
            pltpu.VMEM((lanes, n, rows, rc), bf16),
            pltpu.VMEM((rows, cin), f32),
            dma((4,)),
            dma((6, n, 2)), dma((6, n, 2)), dma((6, n, 2)), dma((6, n, 2)),
            dma((lanes,)), dma((lanes,)), dma((lanes,)), dma((lanes,)),
            dma((lanes,)), dma((lanes,)), dma((lanes, n)), dma((lanes, n)),
        ],
        compiler_params=pltpu.CompilerParams(
            collective_id=0, has_side_effects=True, vmem_limit_bytes=67043328
        ),
    )(tokens, gains, pool_scale[None], gain_out[None], w_in, w_pool_out, w_ff1, w_ff2)


def solution(mesh):
    n, tps = mesh.shape["fs"] // 2, mesh.shape["tp"]
    return jax.shard_map(
        functools.partial(local, n, tps),
        mesh=mesh,
        in_specs=(
            P("fs", "tp"),
            P("tp"),
            P("fs", "tp"),
            P("tp"),
            P("fs", "tp"),
            P("tp"),
            P("fs", "tp"),
            P("fs", "tp"),
            P("tp"),
        ),
        out_specs=P("fs", "tp"),
        check_vma=False,
    )
```

time: 510 us -> 212 us (0.42)
  waiting for transfers between devices: 444 us -> 0 us
  Pallas kernels: 0 us -> 207 us
  matrix products: 26 us -> 0 us
  blocking collectives: 15.7 us -> 0 us
  between operations: 13.6 us -> 0.01 us
  other arithmetic: 10 us -> 1.29 us
    all_gather x6 -> x0, waiting for transfers between devices: 391 us -> none  [the longest x1 128 us: local(): up_full = lax.all_gather(w_ff1, 'fs', axis=0, tiled=True)]
    pallas_call x0 -> x1, Pallas kernels: none -> 207 us  [local(): pl.pallas_call(functools.partial(kernel, n, tps), out_shape=jax.ShapeDtyp...]
    reduce_scatter x2 -> x0, waiting for transfers between devices: 49.4 us -> none  [the longest x1 25 us: local(): lax.psum_scatter(project_rows(out_full, pooled).astype(jnp.bfloat16), 'tp...]
    dot_general x3 -> x0, matrix products: 26 us -> none  [the longest x2 23 us: project_rows(): lax.dot_general(weight, left, (((1,), (1,)), ((), ())), preferred_element...]
    psum x3 -> x0, blocking collectives: 15.7 us -> none  [row_norm(): lax.psum((jnp.sum(value, axis=1), jnp.sum(value * value, axis=1)), 'tp')]
  transfers between devices with their start and end apart: 8 -> 0, of which waited for: 8 -> 0; matrix products, arithmetic and copies ran while one was open for 1% -> 0% of each run, Pallas kernels for 0% -> 0%
where the time goes in v1:
time: 212 us
  Pallas kernels  207 us (98%)
  local copies, waits for them, and re-layouts  2.75 us (1%)
    pallas_call x1, Pallas kernels, local(): pl.pallas_call(functools.partial(kernel, n, tps), out_shape=jax.ShapeDtyp...  207 us

profile of v1, /device:TPU:0, one launch (start us, length us, event | category | flops | bytes accessed | tf_op | source)
XLA Modules:
  0.0 211.5 jit_solution(17277805409856340715)
XLA Ops:
  0.0 0.0 copy-start
  0.0 0.7 copy-done
  0.7 1.3 pad_maximum_fusion.gains_ref
  2.0 207.5 %shard_map.91 = bf16[384,1024]{1,0:T(8,128)(2,1)} custom-call(bf16[384,1024]{1,0:T(8,128)(2,1)} %x_ref.1, f32[2,1024]{1,0:T(2,128)} %pad_maximum_fusion.gains_ref, f32[1,512]{1,0:T(1,128)} %bitcast.7, f32[1,1024]{1,0:T(1,128)} %bitcast.6, bf16[128,512]{1,0:T(8,128)(2,1)} %win_ref.1, bf16[128,512]{1,0:T(8,128)(2,1)} %wpo_ref.1, bf16[128,4096]{1,0:T(8,128)(2,1)} %wup_ref.1, ...), custom_call_target="tpu_custom_call" | custom-call | tf_op jit(solution)/shard_map/pallas_call | solution.py:347
  209.5 2.1 copy.11
Async XLA Ops:
  0.0 0.7 copy-start

commit v2 on v1

--- a/solution.py
+++ b/solution.py
@@ -120,13 +120,25 @@
     for q in range(tps - 1):
         x_copy(q).start()
         g_copy(q).start()
+    loads[2].wait()
+    begin(2)
     xfull[t] = x_ref[...]
     gfull[t] = gains_ref[...]
 
-    run((0, 1), 0, n - 2)
-    loads[2].wait()
-    begin(2)
+    advance((0, 1), 0)
     begin(3)
+
+    pairs = (n - 3) // 2
+
+    def both(s, carry):
+        advance((0, 1), 2 * s + 1)
+        advance((2,), s)
+        advance((0, 1), 2 * s + 2)
+        advance((3,), s)
+        return carry
+
+    lax.fori_loop(0, pairs, both, 0)
+    run((0, 1), 2 * pairs + 1, n - 2)
     advance((0, 1), n - 2, last=True)
     loads[3].wait()
 
@@ -199,7 +211,7 @@
     for q in range(tps - 1):
         m_copy(q).start()
 
-    run((2, 3), 0, half)
+    run((2, 3), pairs, min(half + 2, n - 2))
     for q in range(tps - 1):
         m_copy(q).wait_recv()
 
@@ -217,7 +229,7 @@
             middle[rs, r * feat:(r + 1) * feat] = (pieces[r] * gfull[r, 1:2, :]).astype(bf16)
 
     blocks_of(second_norm)
-    run((2, 3), half, n - 2)
+    run((2, 3), min(half + 2, n - 2), n - 2)
     begin(4)
     begin(5)
     advance((2, 3), n - 2, last=True)
@@ -245,39 +257,29 @@
             part.at[k], precv.at[q, k], ps_sem.at[q, k], pr_sem.at[q, k],
             device_id=(i, peers[q]), device_id_type=MESH)
 
-    def down(distance):
+    def down(s):
         for w in (4, 5):
-            share(w, distance, 0).wait_recv()
-            share(w, lax.rem(n - distance, n), 1).wait_recv()
-        k = chip_at(pos - distance)
-        part[k] = nt_dot(hidden[...], wdn[pl.ds(pl.multiple_of(k * rc, rc), rc), :]).astype(bf16)
+            for d in range(2):
+                share(w, s, d).wait_recv()
+        pieces = []
+        for d in range(2):
+            for c in range(2):
+                r0 = pl.multiple_of((source(s, d) * 2 + c) * own + d * rh, rh)
+                pieces.append(wdn[pl.ds(r0, rh), :])
+        part[s] = nt_dot(hidden[...], jnp.concatenate(pieces, axis=0)).astype(bf16)
         for q in range(tps - 1):
-            p_copy(q, k).start()
-
-    advance((4, 5), 1)
-    run((4, 5), 2, half - 1)
-
-    def first_two(j, carry):
-        down(j * half)
-        return carry
-
-    def last_two(s):
-        def body(j, carry):
-            down(jnp.where(j == 0, s + 1, n - 1 - s))
-            return carry
-        lax.fori_loop(0, 2, body, 0)
-
-    advance((4, 5), half - 1)
-    lax.fori_loop(0, 2, first_two, 0)
+            p_copy(q, s).start()
 
     def tail(s, carry):
         advance((4, 5), s)
-        last_two(s)
+        down(s)
         return carry
 
-    lax.fori_loop(half, n - 2, tail, 0)
+    down(0)
+    lax.fori_loop(1, n - 2, tail, 0)
+    down(n - 2)
     advance((4, 5), n - 2, last=True)
-    last_two(n - 2)
+    down(n - 1)
 
     for q in range(tps - 1):
         def arrived(k, carry):
@@ -291,9 +293,17 @@
         total = jnp.zeros((rb, 1), f32)
         values = []
         for k in range(n):
-            ff = part[k, rs, :].astype(f32)
-            for q in range(tps - 1):
-                ff = ff + precv[q, k, rs, :].astype(f32)
+            at = k // 2 if k % 2 == 0 else n - 1 - k // 2
+            sides = []
+            for d in range(2):
+                s = lax.rem((pos - at if d == 0 else at - pos) + n, n)
+                cs = slice(d * own, (d + 1) * own)
+                ff = part[s, rs, cs].astype(f32)
+                for q in range(tps - 1):
+                    ff = ff + precv[q, s, rs, cs].astype(f32)
+                sides.append(ff)
+            ff = jnp.concatenate(
+                [sides[d][:, c * rh:(c + 1) * rh] for c in range(2) for d in range(2)], axis=1)
             v = residual_alpha * middle[rs, k * rc:(k + 1) * rc].astype(f32) + ff.astype(bf16).astype(f32)
             values.append(v)
             total = total + jnp.sum(v, axis=1, keepdims=True)

time: 212 us -> 214 us (level)
  no operation moved by 1% of the time
where the time goes in v2:
time: 214 us; the launch traced here: 213 us
  Pallas kernels  209 us (98%)
  local copies, waits for them, and re-layouts  2.75 us (1%)
    pallas_call x1, Pallas kernels, local(): pl.pallas_call(functools.partial(kernel, n, tps), out_shape=jax.ShapeDtyp...  209 us

profile of v2, /device:TPU:0, one launch (start us, length us, event | category | flops | bytes accessed | tf_op | source)
XLA Modules:
  0.0 213.2 jit_solution(4722080597094777049)
XLA Ops:
  0.0 0.0 copy-start
  0.0 0.7 copy-done
  0.7 1.3 pad_maximum_fusion.gains_ref
  2.0 209.1 %shard_map.91 = bf16[384,1024]{1,0:T(8,128)(2,1)} custom-call(bf16[384,1024]{1,0:T(8,128)(2,1)} %x_ref.1, f32[2,1024]{1,0:T(2,128)} %pad_maximum_fusion.gains_ref, f32[1,512]{1,0:T(1,128)} %bitcast.7, f32[1,1024]{1,0:T(1,128)} %bitcast.6, bf16[128,512]{1,0:T(8,128)(2,1)} %win_ref.1, bf16[128,512]{1,0:T(8,128)(2,1)} %wpo_ref.1, bf16[128,4096]{1,0:T(8,128)(2,1)} %wup_ref.1, ...), custom_call_target="tpu_custom_call" | custom-call | tf_op jit(solution)/shard_map/pallas_call | solution.py:357
  211.1 2.1 copy.11
Async XLA Ops:
  0.0 0.7 copy-start
